TPU v7x, 256 devices: a whole 4x4x8 slice. The times are simulated.
256 devices in a mesh: ep: 64 (over z, x, core), tp: 4 (over y).
Axes of the slice: x: 4, y: 4, z: 8, core: 2. Of those that a mesh axis runs over, the one named last changes fastest.
Arguments:
- mix_bgate: bfloat16 [16384, 1024], P('ep', 'tp'), may hold values from -6 to 6
- mix_cgate: bfloat16 [16384, 1024], P('ep', 'tp'), may hold values from -6 to 6
- mix_input: bfloat16 [16384, 1024], P('ep', 'tp'), may hold values from -6 to 6
- conv_taps: float32 [3, 1024], P(None, 'tp'), may hold values from -3.5 to 3.5
- mix_out_w: bfloat16 [1024, 2048], P('tp'), may hold values from -0.1875 to 0.1875
- moe_x: bfloat16 [16384, 2048], P('ep', 'tp'), may hold values from -6 to 6
- moe_gain: float32 [2048], replicated, may hold values from 0.1 to 1.9
- routes: int32 [16384, 2], P('ep'), may hold values from 0 to 63, all different within a row; in each aligned block of 256 rows (0 to 255, 256 to 511, ...) at most 12 rows name the same one
- route_w: float32 [16384, 2], P('ep'), may hold values from 0.2 to 1
- w_gate: bfloat16 [64, 2048, 3584], P('ep', None, 'tp'), may hold values from -0.125 to 0.125
- w_up: bfloat16 [64, 2048, 3584], P('ep', None, 'tp'), may hold values from -0.125 to 0.125
- w_down: bfloat16 [64, 3584, 2048], P('ep', 'tp'), may hold values from -0.09375 to 0.09375
Outputs:
- mixed: bfloat16 [16384, 2048], P(('ep', 'tp'))
- routed: bfloat16 [16384, 2048], P('ep', 'tp')
Inputs may be any that keep to these rules, and one draw needn't show every extreme that they name: `routes`: among the 256 rows of one index of ep, each row names 2 different experts and no expert is named by more than 12 rows; in every draw some expert is named by exactly 12 rows of some index.
All inputs are finite; a program needn't handle non-finite values.
Results may differ from a plain program's by a relative error of at most 0.012.
Values may be sent and summed in bfloat16 or wider, within the bound.
A program may use at most 64 MiB of HBM per device.

v0:
```python
import jax
import jax.numpy as jnp
from jax import lax
from jax.sharding import PartitionSpec as P


def shifted(block, axis, distance):
    devices = range(lax.axis_size(axis))
    route = [(i - distance, i) for i in devices if i - distance in devices]
    return lax.ppermute(block, axis, route)


def cut_along(array, dim, devices):
    before, after = (array.shape[:dim], array.shape[dim + 1 :])
    return jnp.moveaxis(array.reshape(*before, devices, -1, *after), dim, 0)


def sent_and_summed(array, axis, dim):
    pieces = cut_along(array, dim, lax.axis_size(axis))
    arrived = lax.all_to_all(pieces, axis, split_axis=0, concat_axis=0, tiled=True)
    return arrived.astype(jnp.float32).sum(axis=0)


def in_order(pieces, dim):
    pieces = jnp.moveaxis(pieces, 0, dim)
    lengths = pieces.shape
    return pieces.reshape(*lengths[:dim], lengths[dim] * lengths[dim + 1], *lengths[dim + 2 :])


def copy_for_each(array, axis):
    copies = jnp.broadcast_to(array, (lax.axis_size(axis), *array.shape))
    return lax.all_to_all(copies, axis, split_axis=0, concat_axis=0, tiled=True)


def gather_directly(array, axis, dim):
    return in_order(copy_for_each(array, axis), dim)


def rms_rows(values, gain):
    wide = values.astype(jnp.float32)
    scale = lax.rsqrt(jnp.mean(wide * wide, axis=-1, keepdims=True) + 1e-06)
    return (wide * scale * gain).astype(jnp.bfloat16)


def conv_mixer(mix_bgate, mix_cgate, mix_input, conv_taps, mix_out_w):
    length = mix_input.shape[0]
    reach = conv_taps.shape[0] - 1
    tail = jnp.stack([mix_cgate[length - reach :], mix_input[length - reach :]])
    before = shifted(tail, "ep", 1)
    gates_c = jnp.concatenate([before[0], mix_cgate], 0).astype(jnp.float32)
    inputs_h = jnp.concatenate([before[1], mix_input], 0).astype(jnp.float32)
    prod = gates_c * inputs_h
    conv = conv_taps[0] * prod[0:length]
    for j in range(1, reach + 1):
        conv = conv + conv_taps[j] * prod[j : j + length]
    gated = (mix_bgate.astype(jnp.float32) * conv).astype(jnp.bfloat16)
    return sent_and_summed(
        jnp.dot(gated, mix_out_w, preferred_element_type=jnp.float32).astype(jnp.bfloat16), "tp", 0
    ).astype(jnp.bfloat16)


def expert_layer(moe_x, moe_gain, routes, route_w, w_gate, w_up, w_down):
    whole = gather_directly(moe_x, "tp", 1)
    normed = rms_rows(whole, moe_gain)
    ntok, width = normed.shape
    top = routes.shape[1]
    n_ep = lax.axis_size("ep")
    n_tp = lax.axis_size("tp")
    per_dev = w_gate.shape[0]
    experts = per_dev * n_ep
    cap = 4 * ((3 * ntok * top + 8 * experts - 1) // (8 * experts))
    flat = routes.reshape(-1)
    onehot = (flat[:, None] == jnp.arange(experts, dtype=jnp.int32)[None, :]).astype(jnp.int32)
    earlier = jnp.cumsum(onehot, axis=0) - onehot
    slot = jnp.sum(earlier * onehot, axis=1)
    place = flat * cap + slot
    source = (
        jnp.full((experts * cap,), ntok, jnp.int32)
        .at[place]
        .set(jnp.arange(ntok * top, dtype=jnp.int32) // top)
    )
    padded = jnp.concatenate([normed, jnp.zeros((1, width), jnp.bfloat16)], 0)
    outgoing = padded[source].reshape(n_ep, per_dev, cap, width)
    part = cap // n_tp
    mine = lax.dynamic_slice_in_dim(outgoing, lax.axis_index("tp") * part, part, 2)
    landed = lax.all_to_all(mine, "ep", split_axis=0, concat_axis=0, tiled=True)
    arrived = gather_directly(landed, "tp", 2)
    gate = jnp.einsum("secd,edf->secf", arrived, w_gate, preferred_element_type=jnp.float32)
    upper = jnp.einsum("secd,edf->secf", arrived, w_up, preferred_element_type=jnp.float32)
    hidden = (jax.nn.silu(gate) * upper).astype(jnp.bfloat16)
    down = jnp.einsum("secf,efd->secd", hidden, w_down, preferred_element_type=jnp.float32)
    summed = sent_and_summed(down.astype(jnp.bfloat16), "tp", 3).astype(jnp.bfloat16)
    returned = lax.all_to_all(summed, "ep", split_axis=0, concat_axis=0, tiled=True)
    flat_back = returned.reshape(experts * cap, width // n_tp)
    picked = flat_back[place].astype(jnp.float32).reshape(ntok, top, width // n_tp)
    return jnp.sum(picked * route_w[:, :, None], axis=1).astype(jnp.bfloat16)


def body(
    mix_bgate,
    mix_cgate,
    mix_input,
    conv_taps,
    mix_out_w,
    moe_x,
    moe_gain,
    routes,
    route_w,
    w_gate,
    w_up,
    w_down,
):
    mixed = conv_mixer(mix_bgate, mix_cgate, mix_input, conv_taps, mix_out_w)
    routed = expert_layer(moe_x, moe_gain, routes, route_w, w_gate, w_up, w_down)
    return (mixed, routed)


def solution(mesh):
    in_specs = (
        P("ep", "tp"),
        P("ep", "tp"),
        P("ep", "tp"),
        P(None, "tp"),
        P("tp", None),
        P("ep", "tp"),
        P(),
        P("ep", None),
        P("ep", None),
        P("ep", None, "tp"),
        P("ep", None, "tp"),
        P("ep", "tp", None),
    )
    out_specs = (P(("ep", "tp"), None), P("ep", "tp"))
    return jax.shard_map(body, mesh=mesh, in_specs=in_specs, out_specs=out_specs, check_vma=False)
```

profile of v0, /device:TPU:1, one launch (start us, length us, event | category | flops | bytes accessed | tf_op | source)
XLA Modules:
  0.0 241.2 jit_solution(3519818174903025259)
XLA Ops:
  0.7 2.1 broadcast_in_dim.8
  2.8 5.0 %all-to-all-start.1 = ((bf16[4,256,512]{2,1,0:T(8,128)(2,1)}), bf16[4,256,512]{2,1,0:T(8,128)(2,1)S(1)}, u32[]{:S(2)}, u32[]{:S(2)}) async-start(bf16[4,256,512]{2,1,0:T(8,128)(2,1)} %broadcast_in_dim.8), calls=%async_computation.1 | async-start | bytes 2097152 | tf_op jit(solution)/shard_map/all_to_all | solution.py:32
  8.2 1.2 reduce-window.6
  10.2 2.4 %scatter_custom_fusion = s32[768]{0:T(1024)S(1)} fusion(s32[512]{0:T(512)S(1)} %bitcast.124, s32[512]{0:T(512)S(1)} %add_select_fusion, s32[]{:T(128)} %constant.42.clone.1), kind=kCustom, calls=%fused_computation.57 | custom fusion | bytes 3076 | tf_op jit(solution)/shard_map/scatter | solution.py:80
  12.6 8.6 %all-to-all-done.1 = bf16[4,256,512]{2,1,0:T(8,128)(2,1)S(1)} async-done(((bf16[4,256,512]{2,1,0:T(8,128)(2,1)}), bf16[4,256,512]{2,1,0:T(8,128)(2,1)S(1)}, u32[]{:S(2)}, u32[]{:S(2)}) %all-to-all-start.1) | async-done | bytes 1048608 | tf_op jit(solution)/shard_map/all_to_all | solution.py:32
  21.8 0.3 fusion.13
  22.6 4.3 %gather_fusion = bf16[768,2048]{1,0:T(8,128)(2,1)} fusion(bf16[257,2048]{1,0:T(8,128)(2,1)S(1)} %concatenate.11, s32[1024]{0:T(1024)S(1)} %pad_clamp_fusion.1), kind=kCustom, calls=%fused_computation | custom fusion | bytes 6294528 | tf_op jit(solution)/shard_map/gather | solution.py:83
  26.9 6.1 %reshape.106 = bf16[64,1,12,2048]{3,2,0,1:T(8,128)(2,1)} reshape(bf16[768,2048]{1,0:T(8,128)(2,1)} %gather_fusion) | data formatting | bytes 6291456 | tf_op jit(solution)/shard_map/reshape | solution.py:83
  33.0 3.0 %dynamic-slice_bitcast_fusion = bf16[64,1,3,2048]{3,2,1,0:T(4,128)(2,1)S(1)} fusion(bf16[64,1,12,2048]{3,2,0,1:T(8,128)(2,1)} %reshape.106, s32[]{:T(128)S(6)} %select_n.25), kind=kLoop, calls=%fused_computation.25 | loop fusion | bytes 1572868 | tf_op jit(solution)/shard_map/dynamic_slice | solution.py:85
  36.0 42.0 %all_to_all.33 = bf16[64,1,3,2048]{3,2,1,0:T(4,128)(2,1)S(1)} all-to-all(bf16[64,1,3,2048]{3,2,1,0:T(4,128)(2,1)S(1)} %dynamic-slice_bitcast_fusion), channel_id=1, replica_groups=mesh['ep'=64,'tp'=4] {'ep'}, dimensions={0} | all-to-all | bytes 1572864 | tf_op jit(solution)/shard_map/all_to_all | solution.py:86
  78.0 0.6 copy.28
  78.6 0.4 broadcast_in_dim.22
  79.0 39.3 %all_to_all.34 = bf16[4,64,1,3,2048]{4,1,3,2,0:T(8,128)(2,1)S(1)} all-to-all(bf16[4,64,1,3,2048]{4,1,3,2,0:T(8,128)(2,1)S(1)} %broadcast_in_dim.22), channel_id=1, replica_groups=mesh['ep'=64,'tp'=4] {'tp'}, dimensions={0} | all-to-all | bytes 6291456 | tf_op jit(solution)/shard_map/all_to_all | solution.py:32
  118.3 1.7 copy-done.1
  120.0 5.0 %fusion.2 = f32[64,12,896]{2,0,1:T(8,128)} fusion(bf16[64,12,2048]{2,0,1:T(8,128)(2,1)S(1)} %bitcast.119, bf16[1,2048,896]{2,1,0:T(8,128)(2,1)S(1)} %copy-done.9), kind=kOutput, calls=%fused_computation.5 | convolution fusion | flops 2818572288 | bytes 9568256 | tf_op jit(solution)/shard_map/secd,edf->secf/dot_general | solution.py:89
  125.0 12.2 %fusion.6 = bf16[64,12,2048]{2,0,1:T(8,128)(2,1)} fusion(bf16[1,896,2048]{2,1,0:T(8,128)(2,1)} %param.23, f32[64,12,896]{2,0,1:T(8,128)} %fusion.2, bf16[64,12,2048]{2,0,1:T(8,128)(2,1)} %bitcast.120, bf16[1,2048,896]{2,1,0:T(8,128)(2,1)} %param.21), kind=kOutput, calls=%fused_computation.9 | convolution fusion | flops 5642846208 | bytes 16384000 | tf_op jit(solution)/shard_map/secf,efd->secd/dot_general | solution.py:91
  137.2 4.0 %copy.39 = bf16[1,12,8,4,8,512]{5,4,2,1,0,3:T(8,128)(2,1)} copy(bf16[1,12,8,4,8,512]{5,4,3,2,1,0:T(8,128)(2,1)} %bitcast.121) | data formatting | bytes 6291456 | tf_op jit(solution)/shard_map/reshape | solution.py:15
  141.2 4.8 %all-to-all-start.4 = ((bf16[4,64,1,12,512]{4,1,3,2,0:T(8,128)(2,1)}), bf16[4,64,1,12,512]{4,1,3,2,0:T(8,128)(2,1)}, u32[]{:S(2)}, u32[]{:S(2)}) async-start(bf16[4,64,1,12,512]{4,1,3,2,0:T(8,128)(2,1)} %bitcast.116), calls=%async_computation.4 | async-start | bytes 6291456 | tf_op jit(solution)/shard_map/all_to_all | solution.py:20
  146.1 4.7 %collective-permute-start = (bf16[2,2,256]{2,1,0:T(2,128)(2,1)S(1)}, bf16[2,2,256]{2,1,0:T(2,128)(2,1)S(1)}, u32[]{:S(2)}, u32[]{:S(2)}) collective-permute-start(bf16[2,2,256]{2,1,0:T(2,128)(2,1)S(1)} %pad_maximum_fusion), channel_id=1, source_target_pairs={{0,4},{4,8},{8,12},{12,16},{16,20},{20,24},{24,28},{28,32},{32,36}... | collective-permute-start | bytes 6152 | tf_op jit(solution)/shard_map/ppermute | solution.py:10
  150.8 0.5 collective-permute-done
  151.4 1.5 convolution_convert_fusion
  152.9 28.9 %all-to-all-done.4 = bf16[4,64,1,12,512]{4,1,3,2,0:T(8,128)(2,1)} async-done(((bf16[4,64,1,12,512]{4,1,3,2,0:T(8,128)(2,1)}), bf16[4,64,1,12,512]{4,1,3,2,0:T(8,128)(2,1)}, u32[]{:S(2)}, u32[]{:S(2)}) %all-to-all-start.4) | async-done | bytes 3145760 | tf_op jit(solution)/shard_map/all_to_all | solution.py:20
  181.8 3.5 %all-to-all-start = ((bf16[4,64,2048]{2,1,0:T(8,128)(2,1)}), bf16[4,64,2048]{2,1,0:T(8,128)(2,1)S(1)}, u32[]{:S(2)}, u32[]{:S(2)}) async-start(bf16[4,64,2048]{2,1,0:T(8,128)(2,1)} %bitcast.7), calls=%async_computation | async-start | bytes 2097152 | tf_op jit(solution)/shard_map/all_to_all | solution.py:20
  185.3 2.5 %reduce_sum.59 = bf16[64,12,512]{2,0,1:T(8,128)(2,1)S(1)} reduce(bf16[4,64,1,12,512]{4,1,3,2,0:T(8,128)(2,1)} %all-to-all-done.4, bf16[]{:T(256)} %constant.19.clone.1), dimensions={0,2}, to_apply=%region_6.7 | reduce | flops 1179648 | bytes 3932162 | tf_op jit(solution)/shard_map/reduce_sum | solution.py:21
  187.8 1.4 copy.31
  189.2 8.1 %all-to-all-done = bf16[4,64,2048]{2,1,0:T(8,128)(2,1)S(1)} async-done(((bf16[4,64,2048]{2,1,0:T(8,128)(2,1)}), bf16[4,64,2048]{2,1,0:T(8,128)(2,1)S(1)}, u32[]{:S(2)}, u32[]{:S(2)}) %all-to-all-start) | async-done | bytes 1048608 | tf_op jit(solution)/shard_map/all_to_all | solution.py:20
  197.3 10.9 %all-to-all-start.5 = ((bf16[64,1,12,512]{3,2,1,0:T(8,128)(2,1)}), bf16[64,1,12,512]{3,2,1,0:T(8,128)(2,1)S(1)}, u32[]{:S(2)}, u32[]{:S(2)}) async-start(bf16[64,1,12,512]{3,2,1,0:T(8,128)(2,1)} %copy.31), calls=%async_computation.5 | async-start | bytes 2097152 | tf_op jit(solution)/shard_map/all_to_all | solution.py:93
  208.3 0.9 reduce_sum.55
  209.2 27.1 %all-to-all-done.5 = bf16[64,1,12,512]{3,2,1,0:T(8,128)(2,1)S(1)} async-done(((bf16[64,1,12,512]{3,2,1,0:T(8,128)(2,1)}), bf16[64,1,12,512]{3,2,1,0:T(8,128)(2,1)S(1)}, u32[]{:S(2)}, u32[]{:S(2)}) %all-to-all-start.5) | async-done | bytes 786464 | tf_op jit(solution)/shard_map/all_to_all | solution.py:93
  236.5 2.0 gather_fusion.1
  238.5 0.7 reshape.115
  239.1 2.1 multiply_reduce_fusion
  (47 shorter events, 2.6 us)
Async XLA Ops:
  0.6 150.7 %copy-start = (bf16[256,2048]{1,0:T(8,128)(2,1)S(1)}, bf16[256,2048]{1,0:T(8,128)(2,1)}, u32[]{:S(2)}) copy-start(bf16[256,2048]{1,0:T(8,128)(2,1)} %param.16) | copy-start | bytes 3145732
  0.6 7.1 %copy-start.6 = (s32[256,2]{0,1:T(2,128)S(1)}, s32[256,2]{0,1:T(2,128)}, u32[]{:S(2)}) copy-start(s32[256,2]{0,1:T(2,128)} %param.19) | copy-start | bytes 6148
  2.8 18.5 %all-to-all-start.1 = ((bf16[4,256,512]{2,1,0:T(8,128)(2,1)}), bf16[4,256,512]{2,1,0:T(8,128)(2,1)S(1)}, u32[]{:S(2)}, u32[]{:S(2)}) async-start(bf16[4,256,512]{2,1,0:T(8,128)(2,1)} %broadcast_in_dim.8), calls=%async_computation.1 | async-start | bytes 2097152 | tf_op jit(solution)/shard_map/all_to_all | solution.py:32
  21.6 0.7 copy-start.5
  79.0 41.0 %copy-start.9 = (bf16[1,2048,896]{2,1,0:T(8,128)(2,1)S(1)}, bf16[1,2048,896]{2,1,0:T(8,128)(2,1)}, u32[]{:S(2)}) copy-start(bf16[1,2048,896]{2,1,0:T(8,128)(2,1)} %param.22) | copy-start | bytes 11010052
  118.3 1.7 copy-start.1
  141.2 4.8 %copy-start.2 = (bf16[256,256]{1,0:T(8,128)(2,1)S(1)}, bf16[256,256]{1,0:T(8,128)(2,1)}, u32[]{:S(2)}) copy-start(bf16[256,256]{1,0:T(8,128)(2,1)} %param.13) | copy-start | bytes 393220
  141.2 4.8 %copy-start.3 = (bf16[256,256]{1,0:T(8,128)(2,1)S(1)}, bf16[256,256]{1,0:T(8,128)(2,1)}, u32[]{:S(2)}) copy-start(bf16[256,256]{1,0:T(8,128)(2,1)} %param.14) | copy-start | bytes 393220
  141.2 9.5 %copy-start.7 = (f32[3,256]{1,0:T(4,128)S(1)}, f32[3,256]{1,0:T(4,128)}, u32[]{:S(2)}) copy-start(f32[3,256]{1,0:T(4,128)} %param.15) | copy-start | bytes 9220
  141.2 10.1 %copy-start.4 = (bf16[256,256]{1,0:T(8,128)(2,1)S(1)}, bf16[256,256]{1,0:T(8,128)(2,1)}, u32[]{:S(2)}) copy-start(bf16[256,256]{1,0:T(8,128)(2,1)} %param.12) | copy-start | bytes 393220
  141.2 40.5 %all-to-all-start.4 = ((bf16[4,64,1,12,512]{4,1,3,2,0:T(8,128)(2,1)}), bf16[4,64,1,12,512]{4,1,3,2,0:T(8,128)(2,1)}, u32[]{:S(2)}, u32[]{:S(2)}) async-start(bf16[4,64,1,12,512]{4,1,3,2,0:T(8,128)(2,1)} %bitcast.116), calls=%async_computation.4 | async-start | bytes 6291456 | tf_op jit(solution)/shard_map/all_to_all | solution.py:20
  146.1 5.2 %collective-permute-start = (bf16[2,2,256]{2,1,0:T(2,128)(2,1)S(1)}, bf16[2,2,256]{2,1,0:T(2,128)(2,1)S(1)}, u32[]{:S(2)}, u32[]{:S(2)}) collective-permute-start(bf16[2,2,256]{2,1,0:T(2,128)(2,1)S(1)} %pad_maximum_fusion), channel_id=1, source_target_pairs={{0,4},{4,8},{8,12},{12,16},{16,20},{20,24},{24,28},{28,32},{32,36}... | collective-permute-start | bytes 6152 | tf_op jit(solution)/shard_map/ppermute | solution.py:10
  181.8 15.5 %all-to-all-start = ((bf16[4,64,2048]{2,1,0:T(8,128)(2,1)}), bf16[4,64,2048]{2,1,0:T(8,128)(2,1)S(1)}, u32[]{:S(2)}, u32[]{:S(2)}) async-start(bf16[4,64,2048]{2,1,0:T(8,128)(2,1)} %bitcast.7), calls=%async_computation | async-start | bytes 2097152 | tf_op jit(solution)/shard_map/all_to_all | solution.py:20
  185.3 22.9 %copy-start.8 = (f32[256,2]{0,1:T(2,128)S(1)}, f32[256,2]{0,1:T(2,128)}, u32[]{:S(2)}) copy-start(f32[256,2]{0,1:T(2,128)} %param.20) | copy-start | bytes 6148
  197.3 39.0 %all-to-all-start.5 = ((bf16[64,1,12,512]{3,2,1,0:T(8,128)(2,1)}), bf16[64,1,12,512]{3,2,1,0:T(8,128)(2,1)S(1)}, u32[]{:S(2)}, u32[]{:S(2)}) async-start(bf16[64,1,12,512]{3,2,1,0:T(8,128)(2,1)} %copy.31), calls=%async_computation.5 | async-start | bytes 2097152 | tf_op jit(solution)/shard_map/all_to_all | solution.py:93
where the time goes:
time: 242 us; the launch traced here: 241 us
  blocking collectives  81.3 us (34%)
  waiting for transfers between devices  73.2 us (30%)
  local copies, waits for them, and re-layouts  30.5 us (13%)
  starting transfers between devices  28.8 us (12%)
  matrix products  18.7 us (8%)
  other arithmetic  7.74 us (3%)
    all_to_all x1, blocking collectives, expert_layer(): landed = lax.all_to_all(mine, 'ep', split_axis=0, concat_axis=0, tiled=True)  42 us
    all_to_all x1, blocking collectives, copy_for_each(): return lax.all_to_all(copies, axis, split_axis=0, concat_axis=0, tiled=True)  39.3 us
    all_to_all x2, waiting for transfers between devices, sent_and_summed(): lax.all_to_all(pieces, axis, split_axis=0, concat_axis=0, tiled=True)  37 us
    all_to_all x1, waiting for transfers between devices, expert_layer(): lax.all_to_all(summed, 'ep', split_axis=0, concat_axis=0, tiled=True)  27.1 us
    dot_general x1, matrix products, expert_layer(): jnp.einsum('secf,efd->secd', hidden, w_down, preferred_element_type=jnp.f...  12.2 us
    all_to_all x1, starting transfers between devices, expert_layer(): lax.all_to_all(summed, 'ep', split_axis=0, concat_axis=0, tiled=True)  10.9 us
    all_to_all x1, waiting for transfers between devices, copy_for_each(): return lax.all_to_all(copies, axis, split_axis=0, concat_axis=0, tiled=True)  8.63 us
    all_to_all x2, starting transfers between devices, sent_and_summed(): lax.all_to_all(pieces, axis, split_axis=0, concat_axis=0, tiled=True)  8.29 us
  transfers between devices with their start and end apart: 5, of which 5 were waited for; matrix products, arithmetic and copies ran while one was open for 5% of the time, Pallas kernels for 0%

commit v1 on v0

v1 whole, which is shorter than its diff:
```python
import functools

import jax
import jax.numpy as jnp
from jax import lax
from jax.experimental import pallas as pl
from jax.experimental.pallas import tpu as pltpu
from jax.sharding import PartitionSpec as P

CAP = 12
TP = 4
BF = jnp.bfloat16
F32 = jnp.float32


def iota(shape, dim):
    return lax.broadcasted_iota(jnp.int32, shape, dim)


def to_message(v, groups):
    h = v.shape[1] // 2
    v0 = v[:, :h].reshape(groups // 2, 8, h)
    v1 = v[:, h:].reshape(groups // 2, 8, h)
    low = iota(v0.shape, 1) < 4
    even = jnp.where(low, v0, pltpu.roll(v1, 4, axis=1))
    odd = jnp.where(low, pltpu.roll(v0, 4, axis=1), v1)
    return even, odd


def from_message(m, groups):
    h = m.shape[2]
    pairs = m.reshape(groups // 2, 2, 8, h)
    even, odd = pairs[:, 0], pairs[:, 1]
    low = iota(even.shape, 1) < 4
    v0 = jnp.where(low, even, pltpu.roll(odd, 4, axis=1))
    v1 = jnp.where(low, pltpu.roll(even, 4, axis=1), odd)
    return v0.reshape(groups * 4, h), v1.reshape(groups * 4, h)


def kernel(
    dims,
    bg, cg, ci, taps, mixw, x, gain, routes, rw, wg, wu, wd,
    mixed, routed,
    wg_v, wu_v, wd_v, mw_v, out, G, nrm, PS, R1, FR, ACC, FIN, ret,
    halo, MS, MR1, MF, MACC,
    wsem, halo_s, halo_r, disp_s, disp_r, gd_s, gd_r, gr_s, gr_r,
    r1_s, r1_r, fi_s, fi_r, fa_s, fa_r, back_s, back_r,
    m1_s, m1_r, mi_s, mi_r, ma_s, ma_r,
):
    NZ, NX, order = dims
    S = NX * 2
    H = S // 2
    n_ep = NZ * S
    ntok, DS = x.shape
    h = DS // 2
    rows = S * CAP
    ar = S * 8
    i = lax.axis_index("ep")
    y = lax.axis_index("tp")
    up = lax.rem(y + 1, TP)
    down = lax.rem(y + 3, TP)
    far = lax.rem(y + 2, TP)
    iz, ix, ic = i // S, (i % S) // 2, i % 2
    sides = ((0, up), (1, down))

    def dz_of(c):
        dz = jnp.int32(0)
        for n in range(NZ):
            dz = jnp.where(c == n, order[n], dz)
        return dz

    def target(c, r):
        return (((iz + dz_of(c)) % NZ) * NX + (ix + r // 2) % NX) * 2 + (ic + r % 2) % 2

    def source(c, r):
        return (((iz + NZ - dz_of(c)) % NZ) * NX + (ix + NX - r // 2) % NX) * 2 + (ic + r % 2) % 2

    def remote(src, dst, ssem, rsem, ep=None, tp=None):
        return pltpu.make_async_remote_copy(
            src_ref=src, dst_ref=dst, send_sem=ssem, recv_sem=rsem,
            device_id=(i if ep is None else ep, y if tp is None else tp),
            device_id_type=pl.DeviceIdType.MESH,
        )

    def arrived(ref, sem):
        remote(ref, ref, sem, sem, tp=up).wait_recv()

    def left(ref, sem):
        remote(ref, ref, sem, sem, tp=up).wait_send()

    barrier = pltpu.get_barrier_semaphore()

    @pl.loop(1, n_ep)
    def _(d):
        pl.semaphore_signal(
            barrier, inc=1, device_id=(lax.rem(i + d, n_ep), y), device_id_type=pl.DeviceIdType.MESH
        )

    for _, other in sides:
        pl.semaphore_signal(barrier, inc=1, device_id=(i, other), device_id_type=pl.DeviceIdType.MESH)

    loads = [
        pltpu.make_async_copy(mixw, mw_v, wsem.at[0]),
        pltpu.make_async_copy(wg.at[0], wg_v, wsem.at[1]),
        pltpu.make_async_copy(wu.at[0], wu_v, wsem.at[2]),
        pltpu.make_async_copy(wd.at[0], wd_v, wsem.at[3]),
    ]
    for load in loads:
        load.start()

    e = routes[...]
    dz = (e // S + NZ - iz) & (NZ - 1)
    chunk = jnp.zeros_like(e)
    for n in range(NZ):
        chunk = jnp.where(dz == order[n], n, chunk)
    er = e & (S - 1)
    dx = ((er // 2) + NX - ix) & (NX - 1)
    dc = (er + ic) & 1
    k = chunk * S + dx * 2 + dc
    hot = [iota((n_ep, ntok), 0) == k[q : q + 1] for q in range(2)]
    named = jnp.where(hot[0] | hot[1], 1.0, 0.0).astype(BF)
    before = jnp.where(iota((ntok, ntok), 0) < iota((ntok, ntok), 1), 1.0, 0.0).astype(BF)
    rank = jnp.dot(named, before, preferred_element_type=F32)
    marks = []
    for q in range(2):
        slot = jnp.sum(jnp.where(hot[q], rank, 0.0), axis=0, keepdims=True).astype(jnp.int32)
        kq = k[q : q + 1]
        marks.append(
            (jnp.where(slot < 8, kq * 8 + slot, -1), jnp.where(slot >= 8, kq * 4 + slot - 8, -1))
        )
    ia = iota((n_ep * 8, ntok), 0)
    ib = iota((n_ep * 4, ntok), 0)
    pa = jnp.where((ia == marks[0][0]) | (ia == marks[1][0]), 1.0, 0.0).astype(BF)
    pb = jnp.where((ib == marks[0][1]) | (ib == marks[1][1]), 1.0, 0.0).astype(BF)
    xv = x[...]
    oa = jnp.dot(pa, xv, preferred_element_type=F32).reshape(n_ep, 8, DS).astype(BF)
    out[:, :, :DS] = oa
    even, odd = to_message(jnp.dot(pb, xv, preferred_element_type=F32), n_ep)
    for p in range(n_ep // 2):
        out[2 * p, :, DS:] = even[p].astype(BF)
        out[2 * p + 1, :, DS:] = odd[p].astype(BF)
    G[0, 0, 0] = out[0]

    pl.semaphore_wait(barrier, n_ep - 1 + 2)

    nxt = lax.rem(i + 1, n_ep)
    ntail = cg.shape[0] - 8
    tails = [
        remote(ref.at[pl.ds(ntail, 8)], halo.at[q], halo_s.at[q], halo_r.at[q], ep=nxt)
        for q, ref in enumerate((cg, ci))
    ]
    for tail in tails:
        tail.start()

    @pl.loop(1, n_ep)
    def _(kk):
        c, r = kk // S, kk % S
        remote(out.at[kk], G.at[0, c, r], disp_s, disp_r.at[c], ep=target(c, r)).start()

    loads[0].wait()
    for tail in tails:
        tail.wait_recv()
    prev = halo[0].astype(F32) * halo[1].astype(F32)
    prev = jnp.where(i > 0, prev, 0.0)
    prod = cg[...].astype(F32) * ci[...].astype(F32)
    row = iota(prod.shape, 0)
    back1 = jnp.where(row == 0, prev[7:8], pltpu.roll(prod, 1, axis=0))
    back2 = jnp.where(row == 0, prev[6:7], jnp.where(row == 1, prev[7:8], pltpu.roll(prod, 2, axis=0)))
    tv = taps[...]
    conv = tv[0:1] * back2 + tv[1:2] * back1 + tv[2:3] * prod
    gated = (bg[...].astype(F32) * conv).astype(BF)
    mrows = MS.shape[1]
    mh = mrows // 2
    for q in range(TP):
        MS[q] = jnp.dot(
            gated[q * mrows : (q + 1) * mrows], mw_v[...], preferred_element_type=F32
        ).astype(BF)
    for d, other in sides:
        remote(
            MS.at[far, pl.ds(d * mh, mh)], MR1.at[d], m1_s.at[d], m1_r.at[d], tp=other
        ).start()
        keep = (1 - d) * mh
        remote(
            MS.at[other, pl.ds(keep, mh)], MF.at[d, pl.ds(keep, mh)], mi_s.at[d], mi_r.at[d], tp=other
        ).start()

    def stage_direct(c):
        @pl.when(c == 0)
        def _():
            arrived(G.at[0, 0, pl.ds(1, S - 1)], disp_r.at[0])

        @pl.when(c > 0)
        def _():
            arrived(G.at[0, c], disp_r.at[c])

        for d, other in sides:
            remote(G.at[0, c], G.at[1 + d, c], gd_s.at[d], gd_r.at[d, c], tp=other).start()

    def stage_relay(c):
        for d, other in sides:
            arrived(G.at[1 + d, c], gd_r.at[d, c])
            half = pl.ds(d * H, H)
            remote(G.at[1 + d, c, half], G.at[3, c, half], gr_s.at[d], gr_r.at[d, c], tp=other).start()

    def stage_expert(c):
        for d in range(2):
            arrived(G.at[3, c, pl.ds(d * H, H)], gr_r.at[d, c])
        owners = (y, down, up, far)
        total = jnp.zeros((S, 8, 1), F32)
        total_b = jnp.zeros((S, 8, 1), F32)
        for n in range(TP):
            g = G[n, c].astype(F32)
            a, b = g[:, :, :DS], g[:, :, DS:]
            total = total + jnp.sum(a * a, axis=2, keepdims=True)
            total_b = total_b + jnp.sum(b * b, axis=2, keepdims=True)
        width = DS * TP
        total_b = total_b + pltpu.roll(total_b, 4, axis=1)
        sa = lax.rsqrt(total / width + 1e-06)
        sb = lax.rsqrt(total_b / width + 1e-06)
        for n, owner in enumerate(owners):
            g = G[n, c].astype(F32)
            gn = gain[owner]
            nrm[owner, pl.ds(0, ar), :] = (g[:, :, :DS] * sa).reshape(ar, DS).astype(F32) * gn
            v0, v1 = from_message(g[:, :, DS:] * sb, S)
            nrm[owner, pl.ds(ar, rows - ar), pl.ds(0, h)] = v0 * gn[:, :h]
            nrm[owner, pl.ds(ar, rows - ar), pl.ds(h, h)] = v1 * gn[:, h:]
        lhs = jnp.concatenate([nrm[n].astype(BF) for n in range(TP)], axis=1)
        gate = jnp.dot(lhs, wg_v[...], preferred_element_type=F32)
        upper = jnp.dot(lhs, wu_v[...], preferred_element_type=F32)
        hidden = (gate / (1.0 + jnp.exp(-gate)) * upper).astype(BF)
        for q in range(TP):
            part = jnp.dot(hidden, wd_v[:, q * DS : (q + 1) * DS], preferred_element_type=F32)
            PS[c, q, :, :, pl.ds(0, DS)] = part[:ar].reshape(S, 8, DS).astype(BF)
            even, odd = to_message(part[ar:], S)
            for p in range(H):
                PS[c, q, 2 * p, :, pl.ds(DS, h)] = even[p].astype(BF)
                PS[c, q, 2 * p + 1, :, pl.ds(DS, h)] = odd[p].astype(BF)
        for d, other in sides:
            half, rest = pl.ds(d * H, H), pl.ds((1 - d) * H, H)
            remote(PS.at[c, far, half], R1.at[d, c], r1_s.at[d], r1_r.at[d, c], tp=other).start()
            remote(PS.at[c, other, rest], FR.at[d, c, rest], fi_s.at[d], fi_r.at[d, c], tp=other).start()

    def stage_add(c):
        for d, other in sides:
            half = pl.ds(d * H, H)
            arrived(R1.at[d, c], r1_r.at[d, c])
            ACC[d, c] = (PS[c, other, half].astype(F32) + R1[d, c].astype(F32)).astype(BF)
            remote(ACC.at[d, c], FR.at[d, c, half], fa_s.at[d], fa_r.at[d, c], tp=other).start()

    def stage_back(c):
        for d in range(2):
            arrived(FR.at[d, c, pl.ds((1 - d) * H, H)], fi_r.at[d, c])
            arrived(FR.at[d, c, pl.ds(d * H, H)], fa_r.at[d, c])
        whole = PS[c, y].astype(F32) + FR[0, c].astype(F32) + FR[1, c].astype(F32)
        FIN[c] = whole.astype(BF)

        @pl.when(c == 0)
        def _():
            ret[0, 0] = FIN[0, 0]

        @pl.loop(0, S)
        def _(r):
            @pl.when(c + r > 0)
            def _():
                remote(FIN.at[c, r], ret.at[c, r], back_s, back_r.at[c], ep=source(c, r)).start()

    for load in loads[1:]:
        load.wait()

    @pl.loop(0, NZ + 4)
    def _(t):
        @pl.when(t < NZ)
        def _():
            stage_direct(t)

        @pl.when((t >= 1) & (t < NZ + 1))
        def _():
            stage_relay(t - 1)

        @pl.when((t >= 3) & (t < NZ + 3))
        def _():
            stage_add(t - 3)

        @pl.when(t >= 4)
        def _():
            stage_back(t - 4)

        @pl.when((t >= 2) & (t < NZ + 2))
        def _():
            stage_expert(t - 2)

        @pl.when(t == NZ)
        def _():
            for d, other in sides:
                half = pl.ds(d * mh, mh)
                arrived(MR1.at[d], m1_r.at[d])
                MACC[d] = (MS[other, half].astype(F32) + MR1[d].astype(F32)).astype(BF)
                remote(MACC.at[d], MF.at[d, half], ma_s.at[d], ma_r.at[d], tp=other).start()

    for d in range(2):
        arrived(MF.at[d, pl.ds((1 - d) * mh, mh)], mi_r.at[d])
        arrived(MF.at[d, pl.ds(d * mh, mh)], ma_r.at[d])
    mixed[...] = (MS[y].astype(F32) + MF[0].astype(F32) + MF[1].astype(F32)).astype(BF)

    table = jnp.concatenate(
        [marks[0][0].astype(F32), marks[1][0].astype(F32), marks[0][1].astype(F32), marks[1][1].astype(F32), rw[...]]
        + [jnp.zeros((122, ntok), F32)],
        axis=0,
    )
    cols = jnp.transpose(table)
    ga = iota((ntok, n_ep * 8), 1)
    gb = iota((ntok, n_ep * 4), 1)
    pick = []
    for q in range(2):
        pick.append(
            (
                jnp.where(ga == cols[:, q : q + 1].astype(jnp.int32), 1.0, 0.0).astype(BF),
                jnp.where(gb == cols[:, 2 + q : 3 + q].astype(jnp.int32), 1.0, 0.0).astype(BF),
                cols[:, 4 + q : 5 + q],
            )
        )
    arrived(ret.at[0, pl.ds(1, S - 1)], back_r.at[0])
    for c in range(1, NZ):
        arrived(ret.at[c], back_r.at[c])
    back = ret[...].reshape(n_ep, 8, DS + h)
    ra = back[:, :, :DS].reshape(n_ep * 8, DS)
    b0, b1 = from_message(back[:, :, DS:].astype(F32), n_ep)
    rb = jnp.concatenate([b0, b1], axis=1).astype(BF)
    total = jnp.zeros((ntok, DS), F32)
    for q in range(2):
        row = jnp.dot(pick[q][0], ra, preferred_element_type=F32)
        row = row + jnp.dot(pick[q][1], rb, preferred_element_type=F32)
        total = total + row * pick[q][2]
    routed[...] = total.astype(BF)

    for tail in tails:
        tail.wait_send()
    left(out.at[pl.ds(1, n_ep - 1)], disp_s)
    left(out.at[pl.ds(1, n_ep - 1)], back_s)
    for d in range(2):
        left(G.at[0], gd_s.at[d])
        left(R1.at[0], gr_s.at[d])
        left(R1.at[0], r1_s.at[d])
        left(R1.at[0], fi_s.at[d])
        left(R1.at[0], fa_s.at[d])
        left(MR1.at[0], m1_s.at[d])
        left(MR1.at[0], mi_s.at[d])
        left(MR1.at[0], ma_s.at[d])


def body(mix_bgate, mix_cgate, mix_input, conv_taps, mix_out_w, moe_x, moe_gain, routes, route_w, w_gate, w_up, w_down, *, dims):
    NZ, NX, order = dims
    S = NX * 2
    H = S // 2
    n_ep = NZ * S
    ntok, DS = moe_x.shape
    D = DS * TP
    F = w_gate.shape[2]
    CH = mix_out_w.shape[0]
    ML = DS + DS // 2
    mrows = mix_input.shape[0] // TP
    vmem = pl.BlockSpec(memory_space=pltpu.VMEM)
    anyspace = pl.BlockSpec(memory_space=pl.ANY)
    V = pltpu.VMEM
    dma = pltpu.SemaphoreType.DMA
    return pl.pallas_call(
        functools.partial(kernel, dims),
        name="step",
        out_shape=(
            jax.ShapeDtypeStruct((mrows, D), BF),
            jax.ShapeDtypeStruct((ntok, DS), BF),
        ),
        in_specs=[vmem, vmem, vmem, vmem, anyspace, vmem, vmem, vmem, vmem, anyspace, anyspace, anyspace],
        out_specs=(vmem, vmem),
        scratch_shapes=[
            V((D, F), BF), V((D, F), BF), V((F, D), BF), V((CH, D), BF),
            V((n_ep, 8, ML), BF),
            V((4, NZ, S, 8, ML), BF),
            V((TP, S * CAP, DS), F32),
            V((NZ, TP, S, 8, ML), BF),
            V((2, NZ, H, 8, ML), BF),
            V((2, NZ, S, 8, ML), BF),
            V((2, NZ, H, 8, ML), BF),
            V((NZ, S, 8, ML), BF),
            V((NZ, S, 8, ML), BF),
            V((2, 8, CH), BF),
            V((TP, mrows, D), BF),
            V((2, mrows // 2, D), BF),
            V((2, mrows, D), BF),
            V((2, mrows // 2, D), BF),
            dma((4,)), dma((2,)), dma((2,)),
            dma, dma((NZ,)),
            dma((2,)), dma((2, NZ)), dma((2,)), dma((2, NZ)),
            dma((2,)), dma((2, NZ)), dma((2,)), dma((2, NZ)), dma((2,)), dma((2, NZ)),
            dma, dma((NZ,)),
            dma((2,)), dma((2,)), dma((2,)), dma((2,)), dma((2,)), dma((2,)),
        ],
        compiler_params=pltpu.CompilerParams(
            collective_id=0, has_side_effects=True, vmem_limit_bytes=60 * 1024 * 1024
        ),
    )(
        mix_bgate, mix_cgate, mix_input, conv_taps, mix_out_w, moe_x,
        moe_gain.reshape(TP, 1, DS), routes.T, route_w.T, w_gate, w_up, w_down,
    )


def solution(mesh):
    n_ep = mesh.shape["ep"]
    NZ, NX = (8, n_ep // 16) if n_ep >= 32 else (2, n_ep // 4)
    order = (0, 2, 6, 3, 5, 4, 1, 7) if NZ == 8 else tuple(range(NZ))
    in_specs = (
        P("ep", "tp"), P("ep", "tp"), P("ep", "tp"), P(None, "tp"), P("tp", None), P("ep", "tp"), P(),
        P("ep", None), P("ep", None), P("ep", None, "tp"), P("ep", None, "tp"), P("ep", "tp", None),
    )
    out_specs = (P(("ep", "tp"), None), P("ep", "tp"))
    return jax.shard_map(
        functools.partial(body, dims=(NZ, NX, order)),
        mesh=mesh, in_specs=in_specs, out_specs=out_specs, check_vma=False,
    )
```

time: 242 us -> 94.4 us (0.39)
  Pallas kernels: 0 us -> 90.3 us
  blocking collectives: 81.3 us -> 0 us
  waiting for transfers between devices: 73.2 us -> 0 us
  starting transfers between devices: 28.8 us -> 0 us
  local copies, waits for them, and re-layouts: 30.5 us -> 3.34 us
  matrix products: 18.7 us -> 0 us
  other arithmetic: 7.74 us -> 0 us
    pallas_call x0 -> x1, Pallas kernels: none -> 90.3 us  [body(): pl.pallas_call(functools.partial(kernel, dims), name='step', out_shape=(j...]
    all_to_all x2 -> x0, blocking collectives: 81.3 us -> none  [the longest x1 42 us: expert_layer(): landed = lax.all_to_all(mine, 'ep', split_axis=0, concat_axis=0, tiled=True)]
    all_to_all x4 -> x0, waiting for transfers between devices: 72.7 us -> none  [the longest x2 37 us: sent_and_summed(): lax.all_to_all(pieces, axis, split_axis=0, concat_axis=0, tiled=True)]
    all_to_all x4 -> x0, starting transfers between devices: 24.2 us -> none  [the longest x1 10.9 us: expert_layer(): lax.all_to_all(summed, 'ep', split_axis=0, concat_axis=0, tiled=True)]
    dot_general x3 -> x0, matrix products: 18.7 us -> none  [the longest x1 12.2 us: expert_layer(): jnp.einsum('secf,efd->secd', hidden, w_down, preferred_element_type=jnp.f...]
    reshape x3 -> x0, local copies, waits for them, and re-layouts: 10.3 us -> none  [the longest x1 6.07 us: expert_layer(): outgoing = padded[source].reshape(n_ep, per_dev, cap, width)]
    gather x2 -> x0, local copies, waits for them, and re-layouts: 6.25 us -> none  [the longest x1 4.27 us: expert_layer(): outgoing = padded[source].reshape(n_ep, per_dev, cap, width)]
    reduce_sum x5 -> x0, other arithmetic: 5.86 us -> none  [the longest x2 3.4 us: sent_and_summed(): return arrived.astype(jnp.float32).sum(axis=0)]
  transfers between devices with their start and end apart: 5 -> 0, of which waited for: 5 -> 0; matrix products, arithmetic and copies ran while one was open for 5% -> 0% of each run, Pallas kernels for 0% -> 0%
where the time goes in v1:
time: 94.4 us; the launch traced here: 94.2 us
  Pallas kernels  90.3 us (96%)
  local copies, waits for them, and re-layouts  3.34 us (4%)
    pallas_call x1, Pallas kernels, body(): pl.pallas_call(functools.partial(kernel, dims), name='step', out_shape=(j...  90.3 us
    unnamed x2, local copies, waits for them, and re-layouts  3.34 us

profile of v1, /device:TPU:1, one launch (start us, length us, event | category | flops | bytes accessed | tf_op | source)
XLA Modules:
  0.0 94.2 jit_solution(9456708614811598730)
XLA Ops:
  0.6 90.3 %step.1 = (bf16[64,2048]{1,0:T(8,128)(2,1)}, bf16[256,512]{1,0:T(8,128)(2,1)}) custom-call(bf16[256,256]{1,0:T(8,128)(2,1)} %bg.1, bf16[256,256]{1,0:T(8,128)(2,1)} %cg.1, bf16[256,256]{1,0:T(8,128)(2,1)} %ci.1, f32[3,256]{1,0:T(4,128)} %taps.1, bf16[256,2048]{1,0:T(8,128)(2,1)} %mixw.1, bf16[256,512]{1,0:T(8,128)(2,1)} %x.1, f32[4,1,512]{2,1,0:T(1,128)} %bitcast.3, ...), custom_call_target="tpu_custom_call" | custom-call | tf_op jit(solution)/shard_map/step/pallas_call | solution.py:366
  90.9 1.7 %copy.16 = bf16[64,2048]{1,0:T(8,128)(2,1)} copy(bf16[64,2048]{1,0:T(8,128)(2,1)} %get-tuple-element.4) | data formatting | bytes 524288
  92.6 1.7 %copy.17 = bf16[256,512]{1,0:T(8,128)(2,1)} copy(bf16[256,512]{1,0:T(8,128)(2,1)} %get-tuple-element.5) | data formatting | bytes 524288

commit v2 on v1

--- a/solution.py
+++ b/solution.py
@@ -39,10 +39,11 @@
 
 def kernel(
     dims,
-    bg, cg, ci, taps, mixw, x, gain, routes, rw, wg, wu, wd,
+    bg_h, cg_h, ci_h, taps_h, mixw, x_h, gain_h, routes_h, rw_h, wg, wu, wd,
     mixed, routed,
+    bg, cg, ci, taps, x, gain, routes, rw,
     wg_v, wu_v, wd_v, mw_v, out, G, nrm, PS, R1, FR, ACC, FIN, ret,
-    halo, MS, MR1, MF, MACC,
+    halo, MS, MR1, MF, MACC, pick_a, pick_b,
     wsem, halo_s, halo_r, disp_s, disp_r, gd_s, gd_r, gr_s, gr_r,
     r1_s, r1_r, fi_s, fi_r, fa_s, fa_r, back_s, back_r,
     m1_s, m1_r, mi_s, mi_r, ma_s, ma_r,
@@ -57,23 +58,22 @@
     ar = S * 8
     i = lax.axis_index("ep")
     y = lax.axis_index("tp")
-    up = lax.rem(y + 1, TP)
-    down = lax.rem(y + 3, TP)
-    far = lax.rem(y + 2, TP)
-    iz, ix, ic = i // S, (i % S) // 2, i % 2
+    up = (y + 1) & (TP - 1)
+    down = (y + 3) & (TP - 1)
+    far = (y + 2) & (TP - 1)
+    ic = i & 1
+    ix = (i >> 1) & (NX - 1)
+    iz = i // S
     sides = ((0, up), (1, down))
+
+    def device(dz, dx, dc):
+        return ((((iz + dz) & (NZ - 1)) * NX + ((ix + dx) & (NX - 1))) << 1) + ((ic + dc) & 1)
 
     def dz_of(c):
         dz = jnp.int32(0)
         for n in range(NZ):
             dz = jnp.where(c == n, order[n], dz)
         return dz
-
-    def target(c, r):
-        return (((iz + dz_of(c)) % NZ) * NX + (ix + r // 2) % NX) * 2 + (ic + r % 2) % 2
-
-    def source(c, r):
-        return (((iz + NZ - dz_of(c)) % NZ) * NX + (ix + NX - r // 2) % NX) * 2 + (ic + r % 2) % 2
 
     def remote(src, dst, ssem, rsem, ep=None, tp=None):
         return pltpu.make_async_remote_copy(
@@ -90,32 +90,36 @@
 
     barrier = pltpu.get_barrier_semaphore()
 
-    @pl.loop(1, n_ep)
-    def _(d):
-        pl.semaphore_signal(
-            barrier, inc=1, device_id=(lax.rem(i + d, n_ep), y), device_id_type=pl.DeviceIdType.MESH
+    def greet(ep, tp):
+        pl.semaphore_signal(barrier, inc=1, device_id=(ep, tp), device_id_type=pl.DeviceIdType.MESH)
+
+    for dz in sorted(range(NZ), key=lambda n: -min(n, NZ - n)):
+        for r in range(S):
+            if dz + r:
+                greet(device(dz, r // 2, r % 2), y)
+    for _, other in sides:
+        greet(i, other)
+
+    loads = [
+        pltpu.make_async_copy(src, dst, wsem.at[n])
+        for n, (src, dst) in enumerate(
+            (
+                (routes_h, routes), (x_h, x), (cg_h, cg), (ci_h, ci), (bg_h, bg), (taps_h, taps), (mixw, mw_v),
+                (rw_h, rw), (gain_h, gain), (wg.at[0], wg_v), (wu.at[0], wu_v), (wd.at[0], wd_v),
+            )
         )
-
-    for _, other in sides:
-        pl.semaphore_signal(barrier, inc=1, device_id=(i, other), device_id_type=pl.DeviceIdType.MESH)
-
-    loads = [
-        pltpu.make_async_copy(mixw, mw_v, wsem.at[0]),
-        pltpu.make_async_copy(wg.at[0], wg_v, wsem.at[1]),
-        pltpu.make_async_copy(wu.at[0], wu_v, wsem.at[2]),
-        pltpu.make_async_copy(wd.at[0], wd_v, wsem.at[3]),
     ]
     for load in loads:
         load.start()
 
+    loads[0].wait()
     e = routes[...]
     dz = (e // S + NZ - iz) & (NZ - 1)
     chunk = jnp.zeros_like(e)
     for n in range(NZ):
         chunk = jnp.where(dz == order[n], n, chunk)
-    er = e & (S - 1)
-    dx = ((er // 2) + NX - ix) & (NX - 1)
-    dc = (er + ic) & 1
+    dx = ((e >> 1) + NX - ix) & (NX - 1)
+    dc = (e + ic) & 1
     k = chunk * S + dx * 2 + dc
     hot = [iota((n_ep, ntok), 0) == k[q : q + 1] for q in range(2)]
     named = jnp.where(hot[0] | hot[1], 1.0, 0.0).astype(BF)
@@ -132,6 +136,7 @@
     ib = iota((n_ep * 4, ntok), 0)
     pa = jnp.where((ia == marks[0][0]) | (ia == marks[1][0]), 1.0, 0.0).astype(BF)
     pb = jnp.where((ib == marks[0][1]) | (ib == marks[1][1]), 1.0, 0.0).astype(BF)
+    loads[1].wait()
     xv = x[...]
     oa = jnp.dot(pa, xv, preferred_element_type=F32).reshape(n_ep, 8, DS).astype(BF)
     out[:, :, :DS] = oa
@@ -141,40 +146,48 @@
         out[2 * p + 1, :, DS:] = odd[p].astype(BF)
     G[0, 0, 0] = out[0]
 
+    for load in loads[2:7]:
+        load.wait()
+    mrows = MS.shape[1]
+    mh = mrows // 2
+    prod = cg[...].astype(F32) * ci[...].astype(F32)
+    back1 = pltpu.roll(prod, 1, axis=0)
+    back2 = pltpu.roll(prod, 2, axis=0)
+    tv = taps[...]
+    conv = tv[0:1] * back2 + tv[1:2] * back1 + tv[2:3] * prod
+    gated = (bg[...].astype(F32) * conv).astype(BF)
+    for q in range(1, TP):
+        MS[q] = jnp.dot(
+            gated[q * mrows : (q + 1) * mrows], mw_v[...], preferred_element_type=F32
+        ).astype(BF)
+
     pl.semaphore_wait(barrier, n_ep - 1 + 2)
 
-    nxt = lax.rem(i + 1, n_ep)
     ntail = cg.shape[0] - 8
     tails = [
-        remote(ref.at[pl.ds(ntail, 8)], halo.at[q], halo_s.at[q], halo_r.at[q], ep=nxt)
+        remote(ref.at[pl.ds(ntail, 8)], halo.at[q], halo_s.at[q], halo_r.at[q], ep=(i + 1) & (n_ep - 1))
         for q, ref in enumerate((cg, ci))
     ]
     for tail in tails:
         tail.start()
 
-    @pl.loop(1, n_ep)
-    def _(kk):
-        c, r = kk // S, kk % S
-        remote(out.at[kk], G.at[0, c, r], disp_s, disp_r.at[c], ep=target(c, r)).start()
-
-    loads[0].wait()
+    for c in range(NZ):
+        for r in range(S):
+            if c + r:
+                remote(
+                    out.at[c * S + r], G.at[0, c, r], disp_s, disp_r.at[c], ep=device(order[c], r // 2, r % 2)
+                ).start()
+
     for tail in tails:
         tail.wait_recv()
     prev = halo[0].astype(F32) * halo[1].astype(F32)
     prev = jnp.where(i > 0, prev, 0.0)
-    prod = cg[...].astype(F32) * ci[...].astype(F32)
-    row = iota(prod.shape, 0)
-    back1 = jnp.where(row == 0, prev[7:8], pltpu.roll(prod, 1, axis=0))
-    back2 = jnp.where(row == 0, prev[6:7], jnp.where(row == 1, prev[7:8], pltpu.roll(prod, 2, axis=0)))
-    tv = taps[...]
-    conv = tv[0:1] * back2 + tv[1:2] * back1 + tv[2:3] * prod
-    gated = (bg[...].astype(F32) * conv).astype(BF)
-    mrows = MS.shape[1]
-    mh = mrows // 2
-    for q in range(TP):
-        MS[q] = jnp.dot(
-            gated[q * mrows : (q + 1) * mrows], mw_v[...], preferred_element_type=F32
-        ).astype(BF)
+    row = iota((mrows, prod.shape[1]), 0)
+    first1 = jnp.where(row == 0, prev[7:8], back1[:mrows])
+    first2 = jnp.where(row == 0, prev[6:7], jnp.where(row == 1, prev[7:8], back2[:mrows]))
+    conv = tv[0:1] * first2 + tv[1:2] * first1 + tv[2:3] * prod[:mrows]
+    gated = (bg[pl.ds(0, mrows), :].astype(F32) * conv).astype(BF)
+    MS[0] = jnp.dot(gated, mw_v[...], preferred_element_type=F32).astype(BF)
     for d, other in sides:
         remote(
             MS.at[far, pl.ds(d * mh, mh)], MR1.at[d], m1_s.at[d], m1_r.at[d], tp=other
@@ -184,6 +197,21 @@
             MS.at[other, pl.ds(keep, mh)], MF.at[d, pl.ds(keep, mh)], mi_s.at[d], mi_r.at[d], tp=other
         ).start()
 
+    loads[7].wait()
+    loads[8].wait()
+    table = jnp.concatenate(
+        [marks[0][0].astype(F32), marks[1][0].astype(F32), marks[0][1].astype(F32), marks[1][1].astype(F32), rw[...]]
+        + [jnp.zeros((122, ntok), F32)],
+        axis=0,
+    )
+    cols = jnp.transpose(table)
+    ga = iota((ntok, n_ep * 8), 1)
+    gb = iota((ntok, n_ep * 4), 1)
+    for q in range(2):
+        pick_a[q] = jnp.where(ga == cols[:, q : q + 1].astype(jnp.int32), 1.0, 0.0).astype(BF)
+        pick_b[q] = jnp.where(gb == cols[:, 2 + q : 3 + q].astype(jnp.int32), 1.0, 0.0).astype(BF)
+    share = [cols[:, 4 + q : 5 + q] for q in range(2)]
+
     def stage_direct(c):
         @pl.when(c == 0)
         def _():
@@ -203,6 +231,11 @@
             remote(G.at[1 + d, c, half], G.at[3, c, half], gr_s.at[d], gr_r.at[d, c], tp=other).start()
 
     def stage_expert(c):
+        @pl.when(c == 0)
+        def _():
+            for load in loads[9:]:
+                load.wait()
+
         for d in range(2):
             arrived(G.at[3, c, pl.ds(d * H, H)], gr_r.at[d, c])
         owners = (y, down, up, far)
@@ -258,38 +291,39 @@
         def _():
             ret[0, 0] = FIN[0, 0]
 
-        @pl.loop(0, S)
-        def _(r):
-            @pl.when(c + r > 0)
-            def _():
-                remote(FIN.at[c, r], ret.at[c, r], back_s, back_r.at[c], ep=source(c, r)).start()
-
-    for load in loads[1:]:
-        load.wait()
-
-    @pl.loop(0, NZ + 4)
-    def _(t):
-        @pl.when(t < NZ)
-        def _():
-            stage_direct(t)
-
-        @pl.when((t >= 1) & (t < NZ + 1))
-        def _():
-            stage_relay(t - 1)
-
-        @pl.when((t >= 3) & (t < NZ + 3))
-        def _():
-            stage_add(t - 3)
-
-        @pl.when(t >= 4)
-        def _():
-            stage_back(t - 4)
-
-        @pl.when((t >= 2) & (t < NZ + 2))
-        def _():
-            stage_expert(t - 2)
-
-        @pl.when(t == NZ)
+        dz = NZ - dz_of(c)
+        for r in range(S):
+            send = remote(
+                FIN.at[c, r], ret.at[c, r], back_s, back_r.at[c], ep=device(dz, NX - r // 2, r % 2)
+            )
+            if r:
+                send.start()
+            else:
+                pl.when(c > 0)(send.start)
+
+    @pl.loop(-3, NZ + 2)
+    def _(u):
+        @pl.when((u >= -1) & (u < NZ - 1))
+        def _():
+            stage_relay(u + 1)
+
+        @pl.when(u < NZ - 3)
+        def _():
+            stage_direct(u + 3)
+
+        @pl.when((u >= 1) & (u < NZ + 1))
+        def _():
+            stage_add(u - 1)
+
+        @pl.when(u >= 2)
+        def _():
+            stage_back(u - 2)
+
+        @pl.when((u >= 0) & (u < NZ))
+        def _():
+            stage_expert(u)
+
+        @pl.when(u == NZ - 2)
         def _():
             for d, other in sides:
                 half = pl.ds(d * mh, mh)
@@ -302,23 +336,6 @@
         arrived(MF.at[d, pl.ds(d * mh, mh)], ma_r.at[d])
     mixed[...] = (MS[y].astype(F32) + MF[0].astype(F32) + MF[1].astype(F32)).astype(BF)
 
-    table = jnp.concatenate(
-        [marks[0][0].astype(F32), marks[1][0].astype(F32), marks[0][1].astype(F32), marks[1][1].astype(F32), rw[...]]
-        + [jnp.zeros((122, ntok), F32)],
-        axis=0,
-    )
-    cols = jnp.transpose(table)
-    ga = iota((ntok, n_ep * 8), 1)
-    gb = iota((ntok, n_ep * 4), 1)
-    pick = []
-    for q in range(2):
-        pick.append(
-            (
-                jnp.where(ga == cols[:, q : q + 1].astype(jnp.int32), 1.0, 0.0).astype(BF),
-                jnp.where(gb == cols[:, 2 + q : 3 + q].astype(jnp.int32), 1.0, 0.0).astype(BF),
-                cols[:, 4 + q : 5 + q],
-            )
-        )
     arrived(ret.at[0, pl.ds(1, S - 1)], back_r.at[0])
     for c in range(1, NZ):
         arrived(ret.at[c], back_r.at[c])
@@ -328,9 +345,9 @@
     rb = jnp.concatenate([b0, b1], axis=1).astype(BF)
     total = jnp.zeros((ntok, DS), F32)
     for q in range(2):
-        row = jnp.dot(pick[q][0], ra, preferred_element_type=F32)
-        row = row + jnp.dot(pick[q][1], rb, preferred_element_type=F32)
-        total = total + row * pick[q][2]
+        row = jnp.dot(pick_a[q], ra, preferred_element_type=F32)
+        row = row + jnp.dot(pick_b[q], rb, preferred_element_type=F32)
+        total = total + row * share[q]
     routed[...] = total.astype(BF)
 
     for tail in tails:
@@ -358,21 +375,24 @@
     F = w_gate.shape[2]
     CH = mix_out_w.shape[0]
     ML = DS + DS // 2
-    mrows = mix_input.shape[0] // TP
+    length = mix_input.shape[0]
+    mrows = length // TP
     vmem = pl.BlockSpec(memory_space=pltpu.VMEM)
-    anyspace = pl.BlockSpec(memory_space=pl.ANY)
+    hbm = pl.BlockSpec(memory_space=pltpu.HBM)
     V = pltpu.VMEM
     dma = pltpu.SemaphoreType.DMA
     return pl.pallas_call(
         functools.partial(kernel, dims),
         name="step",
         out_shape=(
-            jax.ShapeDtypeStruct((mrows, D), BF),
-            jax.ShapeDtypeStruct((ntok, DS), BF),
+            V((mrows, D), BF),
+            V((ntok, DS), BF),
         ),
-        in_specs=[vmem, vmem, vmem, vmem, anyspace, vmem, vmem, vmem, vmem, anyspace, anyspace, anyspace],
+        in_specs=[hbm] * 12,
         out_specs=(vmem, vmem),
         scratch_shapes=[
+            V((length, CH), BF), V((length, CH), BF), V((length, CH), BF), V((3, CH), F32),
+            V((ntok, DS), BF), V((TP, 1, DS), F32), V((2, ntok), jnp.int32), V((2, ntok), F32),
             V((D, F), BF), V((D, F), BF), V((F, D), BF), V((CH, D), BF),
             V((n_ep, 8, ML), BF),
             V((4, NZ, S, 8, ML), BF),
@@ -388,7 +408,8 @@
             V((2, mrows // 2, D), BF),
             V((2, mrows, D), BF),
             V((2, mrows // 2, D), BF),
-            dma((4,)), dma((2,)), dma((2,)),
+            V((2, ntok, n_ep * 8), BF), V((2, ntok, n_ep * 4), BF),
+            dma((12,)), dma((2,)), dma((2,)),
             dma, dma((NZ,)),
             dma((2,)), dma((2, NZ)), dma((2,)), dma((2, NZ)),
             dma((2,)), dma((2, NZ)), dma((2,)), dma((2, NZ)), dma((2,)), dma((2, NZ)),
@@ -396,7 +417,7 @@
             dma((2,)), dma((2,)), dma((2,)), dma((2,)), dma((2,)), dma((2,)),
         ],
         compiler_params=pltpu.CompilerParams(
-            collective_id=0, has_side_effects=True, vmem_limit_bytes=60 * 1024 * 1024
+            collective_id=0, has_side_effects=True, vmem_limit_bytes=67043328 - 2 * 2 * mrows * D - 16384
         ),
     )(
         mix_bgate, mix_cgate, mix_input, conv_taps, mix_out_w, moe_x,
@@ -407,7 +428,7 @@
 def solution(mesh):
     n_ep = mesh.shape["ep"]
     NZ, NX = (8, n_ep // 16) if n_ep >= 32 else (2, n_ep // 4)
-    order = (0, 2, 6, 3, 5, 4, 1, 7) if NZ == 8 else tuple(range(NZ))
+    order = (0, 1, 6, 3, 5, 4, 2, 7) if NZ == 8 else tuple(range(NZ))
     in_specs = (
         P("ep", "tp"), P("ep", "tp"), P("ep", "tp"), P(None, "tp"), P("tp", None), P("ep", "tp"), P(),
         P("ep", None), P("ep", None), P("ep", None, "tp"), P("ep", None, "tp"), P("ep", "tp", None),

time: 94.4 us -> 89.4 us (0.947)
  Pallas kernels: 90.3 us -> 87.3 us
  local copies, waits for them, and re-layouts: 3.34 us -> 1.41 us
    pallas_call x1, Pallas kernels: 90.3 us -> 87.3 us  [body(): pl.pallas_call(functools.partial(kernel, dims), name='step', out_shape=(V...]
    unnamed x2, local copies, waits for them, and re-layouts: 3.34 us -> 1.41 us
where the time goes in v2:
time: 89.4 us
  Pallas kernels  87.3 us (98%)
  local copies, waits for them, and re-layouts  1.41 us (2%)
    pallas_call x1, Pallas kernels, body(): pl.pallas_call(functools.partial(kernel, dims), name='step', out_shape=(V...  87.3 us

profile of v2, /device:TPU:1, one launch (start us, length us, event | category | flops | bytes accessed | tf_op | source)
XLA Modules:
  0.0 89.4 jit_solution(3656788402536535014)
XLA Ops:
  0.6 87.3 %step.1 = (bf16[64,2048]{1,0:T(8,128)(2,1)S(1)}, bf16[256,512]{1,0:T(8,128)(2,1)S(1)}) custom-call(bf16[256,256]{1,0:T(8,128)(2,1)} %bg_h.1, bf16[256,256]{1,0:T(8,128)(2,1)} %cg_h.1, bf16[256,256]{1,0:T(8,128)(2,1)} %ci_h.1, f32[3,256]{1,0:T(4,128)} %taps_h.1, bf16[256,2048]{1,0:T(8,128)(2,1)} %mixw.1, bf16[256,512]{1,0:T(8,128)(2,1)} %x_h.1, ...), custom_call_target="tpu_custom_call" | custom-call | tf_op jit(solution)/shard_map/step/pallas_call | solution.py:384
  87.9 0.7 copy.16
  88.6 0.7 copy.17

commit v3 on v2

--- a/solution.py
+++ b/solution.py
@@ -43,12 +43,12 @@
     mixed, routed,
     bg, cg, ci, taps, x, gain, routes, rw,
     wg_v, wu_v, wd_v, mw_v, out, G, nrm, PS, R1, FR, ACC, FIN, ret,
-    halo, MS, MR1, MF, MACC, pick_a, pick_b,
+    halo, MS, MR1, MF, MACC, XS, XR1, XF, XACC, XO, pick_a, pick_b,
     wsem, halo_s, halo_r, disp_s, disp_r, gd_s, gd_r, gr_s, gr_r,
     r1_s, r1_r, fi_s, fi_r, fa_s, fa_r, back_s, back_r,
-    m1_s, m1_r, mi_s, mi_r, ma_s, ma_r,
+    m1_s, m1_r, mi_s, mi_r, ma_s, ma_r, x1_s, x1_r, xi_s, xi_r, xa_s, xa_r, xin_s, xin_r, xo_s, xo_r,
 ):
-    NZ, NX, order = dims
+    NZ, NX, orders = dims
     S = NX * 2
     H = S // 2
     n_ep = NZ * S
@@ -69,11 +69,10 @@
     def device(dz, dx, dc):
         return ((((iz + dz) & (NZ - 1)) * NX + ((ix + dx) & (NX - 1))) << 1) + ((ic + dc) & 1)
 
-    def dz_of(c):
-        dz = jnp.int32(0)
-        for n in range(NZ):
-            dz = jnp.where(c == n, order[n], dz)
-        return dz
+    taken, place = jnp.int32(0), jnp.int32(0)
+    for n in range(NZ):
+        taken = jnp.where(iz == n, sum(p << 4 * c for c, p in enumerate(orders[n])), taken)
+        place = jnp.where(iz == n, sum(orders[e].index(n) << 4 * e for e in range(NZ)), place)
 
     def remote(src, dst, ssem, rsem, ep=None, tp=None):
         return pltpu.make_async_remote_copy(
@@ -115,12 +114,9 @@
     loads[0].wait()
     e = routes[...]
     dz = (e // S + NZ - iz) & (NZ - 1)
-    chunk = jnp.zeros_like(e)
-    for n in range(NZ):
-        chunk = jnp.where(dz == order[n], n, chunk)
     dx = ((e >> 1) + NX - ix) & (NX - 1)
     dc = (e + ic) & 1
-    k = chunk * S + dx * 2 + dc
+    k = dz * S + dx * 2 + dc
     hot = [iota((n_ep, ntok), 0) == k[q : q + 1] for q in range(2)]
     named = jnp.where(hot[0] | hot[1], 1.0, 0.0).astype(BF)
     before = jnp.where(iota((ntok, ntok), 0) < iota((ntok, ntok), 1), 1.0, 0.0).astype(BF)
@@ -148,18 +144,21 @@
 
     for load in loads[2:7]:
         load.wait()
-    mrows = MS.shape[1]
-    mh = mrows // 2
+    groups, more = MS.shape[1], XS.shape[1] // 2
+    mrows = (groups + more) * 8
+    buddy = i + 1 - 2 * ic
     prod = cg[...].astype(F32) * ci[...].astype(F32)
     back1 = pltpu.roll(prod, 1, axis=0)
     back2 = pltpu.roll(prod, 2, axis=0)
     tv = taps[...]
     conv = tv[0:1] * back2 + tv[1:2] * back1 + tv[2:3] * prod
     gated = (bg[...].astype(F32) * conv).astype(BF)
-    for q in range(1, TP):
-        MS[q] = jnp.dot(
-            gated[q * mrows : (q + 1) * mrows], mw_v[...], preferred_element_type=F32
-        ).astype(BF)
+    for q in range(TP):
+        product = jnp.dot(gated[q * mrows : (q + 1) * mrows], mw_v[...], preferred_element_type=F32)
+        product = product.reshape(groups + more, 8, product.shape[1]).astype(BF)
+        if q:
+            MS[q] = product[:groups]
+        XS[q, pl.ds(0, more)] = product[groups:]
 
     pl.semaphore_wait(barrier, n_ep - 1 + 2)
 
@@ -168,14 +167,46 @@
         remote(ref.at[pl.ds(ntail, 8)], halo.at[q], halo_s.at[q], halo_r.at[q], ep=(i + 1) & (n_ep - 1))
         for q, ref in enumerate((cg, ci))
     ]
+    def begin(own, first, last, size, sems, ready):
+        half = size // 2
+        for d, other in sides:
+            keep = (1 - d) * half
+
+            @pl.when(ready(far))
+            def _():
+                remote(
+                    own.at[far, pl.ds(d * half, half)], first.at[d], sems[0].at[d], sems[1].at[d], tp=other
+                ).start()
+
+            @pl.when(ready(other))
+            def _():
+                remote(
+                    own.at[other, pl.ds(keep, half)], last.at[d, pl.ds(keep, half)], sems[2].at[d], sems[3].at[d],
+                    tp=other,
+                ).start()
+
+    m_sems = (m1_s, m1_r, mi_s, mi_r, ma_s, ma_r)
+    x_sems = (x1_s, x1_r, xi_s, xi_r, xa_s, xa_r)
     for tail in tails:
         tail.start()
-
-    for c in range(NZ):
+    begin(MS, MR1, MF, groups, m_sems, lambda q: q > 0)
+
+    handed = [
+        remote(XS.at[q, pl.ds(0, more)], XS.at[q, pl.ds(more, more)], xin_s.at[q], xin_r.at[q], ep=buddy)
+        for q in range(TP)
+    ]
+
+    @pl.when(ic == 0)
+    def _():
+        for hand in handed:
+            hand.start()
+
+    for dz in sorted(range(NZ), key=lambda n: min(n, NZ - n)):
+        c = (place >> (((iz + dz) & (NZ - 1)) * 4)) & 15 if dz else 0
         for r in range(S):
-            if c + r:
+            if dz + r:
                 remote(
-                    out.at[c * S + r], G.at[0, c, r], disp_s, disp_r.at[c], ep=device(order[c], r // 2, r % 2)
+                    out.at[dz * S + r], G.at[0, c, r], disp_s, disp_r.at[c], ep=device(dz, r // 2, r % 2)
                 ).start()
 
     for tail in tails:
@@ -187,15 +218,31 @@
     first2 = jnp.where(row == 0, prev[6:7], jnp.where(row == 1, prev[7:8], back2[:mrows]))
     conv = tv[0:1] * first2 + tv[1:2] * first1 + tv[2:3] * prod[:mrows]
     gated = (bg[pl.ds(0, mrows), :].astype(F32) * conv).astype(BF)
-    MS[0] = jnp.dot(gated, mw_v[...], preferred_element_type=F32).astype(BF)
-    for d, other in sides:
-        remote(
-            MS.at[far, pl.ds(d * mh, mh)], MR1.at[d], m1_s.at[d], m1_r.at[d], tp=other
-        ).start()
-        keep = (1 - d) * mh
-        remote(
-            MS.at[other, pl.ds(keep, mh)], MF.at[d, pl.ds(keep, mh)], mi_s.at[d], mi_r.at[d], tp=other
-        ).start()
+    product = jnp.dot(gated, mw_v[...], preferred_element_type=F32)
+    MS[0] = product.reshape(groups + more, 8, product.shape[1])[:groups].astype(BF)
+
+    def pass_on(own, first, last, added, size, sems):
+        half = size // 2
+        for d, other in sides:
+            part = pl.ds(d * half, half)
+            arrived(first.at[d], sems[1].at[d])
+            added[d] = (own[other, part].astype(F32) + first[d].astype(F32)).astype(BF)
+            remote(added.at[d], last.at[d, part], sems[4].at[d], sems[5].at[d], tp=other).start()
+
+    def summed(own, last, size, sems):
+        half = size // 2
+        for d in range(2):
+            arrived(last.at[d, pl.ds((1 - d) * half, half)], sems[3].at[d])
+            arrived(last.at[d, pl.ds(d * half, half)], sems[5].at[d])
+        return (own[y].astype(F32) + last[0].astype(F32) + last[1].astype(F32)).astype(BF)
+
+    begin(MS, MR1, MF, groups, m_sems, lambda q: q == 0)
+
+    @pl.when(ic == 1)
+    def _():
+        for hand in handed:
+            hand.wait_recv()
+        begin(XS, XR1, XF, 2 * more, x_sems, lambda q: q >= 0)
 
     loads[7].wait()
     loads[8].wait()
@@ -291,10 +338,11 @@
         def _():
             ret[0, 0] = FIN[0, 0]
 
-        dz = NZ - dz_of(c)
+        plane = (taken >> (4 * c)) & 15
+        dz = (iz - plane) & (NZ - 1)
         for r in range(S):
             send = remote(
-                FIN.at[c, r], ret.at[c, r], back_s, back_r.at[c], ep=device(dz, NX - r // 2, r % 2)
+                FIN.at[c, r], ret.at[dz, r], back_s, back_r.at[dz], ep=device(NZ - dz, NX - r // 2, r % 2)
             )
             if r:
                 send.start()
@@ -311,6 +359,10 @@
         def _():
             stage_direct(u + 3)
 
+        @pl.when((u >= 0) & (u < NZ))
+        def _():
+            stage_expert(u)
+
         @pl.when((u >= 1) & (u < NZ + 1))
         def _():
             stage_add(u - 1)
@@ -319,22 +371,29 @@
         def _():
             stage_back(u - 2)
 
-        @pl.when((u >= 0) & (u < NZ))
-        def _():
-            stage_expert(u)
-
         @pl.when(u == NZ - 2)
         def _():
-            for d, other in sides:
-                half = pl.ds(d * mh, mh)
-                arrived(MR1.at[d], m1_r.at[d])
-                MACC[d] = (MS[other, half].astype(F32) + MR1[d].astype(F32)).astype(BF)
-                remote(MACC.at[d], MF.at[d, half], ma_s.at[d], ma_r.at[d], tp=other).start()
-
-    for d in range(2):
-        arrived(MF.at[d, pl.ds((1 - d) * mh, mh)], mi_r.at[d])
-        arrived(MF.at[d, pl.ds(d * mh, mh)], ma_r.at[d])
-    mixed[...] = (MS[y].astype(F32) + MF[0].astype(F32) + MF[1].astype(F32)).astype(BF)
+            pass_on(MS, MR1, MF, MACC, groups, m_sems)
+
+            @pl.when(ic == 1)
+            def _():
+                pass_on(XS, XR1, XF, XACC, 2 * more, x_sems)
+
+    kept = groups * 8
+    mixed[pl.ds(0, kept), :] = summed(MS, MF, groups, m_sems).reshape(kept, -1)
+    result = remote(XO.at[0], XO.at[1], xo_s, xo_r, ep=buddy)
+
+    @pl.when(ic == 1)
+    def _():
+        both = summed(XS, XF, 2 * more, x_sems)
+        XO[0] = both[more:]
+        result.start()
+        mixed[pl.ds(kept, mrows - kept), :] = both[:more].reshape(mrows - kept, -1)
+
+    @pl.when(ic == 0)
+    def _():
+        result.wait_recv()
+        mixed[pl.ds(kept, mrows - kept), :] = XO[1].reshape(mrows - kept, -1)
 
     arrived(ret.at[0, pl.ds(1, S - 1)], back_r.at[0])
     for c in range(1, NZ):
@@ -364,9 +423,22 @@
         left(MR1.at[0], mi_s.at[d])
         left(MR1.at[0], ma_s.at[d])
 
+    @pl.when(ic == 1)
+    def _():
+        result.wait_send()
+        for d in range(2):
+            left(XR1.at[0], x1_s.at[d])
+            left(XR1.at[0], xi_s.at[d])
+            left(XR1.at[0], xa_s.at[d])
+
+    @pl.when(ic == 0)
+    def _():
+        for hand in handed:
+            hand.wait_send()
+
 
 def body(mix_bgate, mix_cgate, mix_input, conv_taps, mix_out_w, moe_x, moe_gain, routes, route_w, w_gate, w_up, w_down, *, dims):
-    NZ, NX, order = dims
+    NZ, NX, _ = dims
     S = NX * 2
     H = S // 2
     n_ep = NZ * S
@@ -377,6 +449,8 @@
     ML = DS + DS // 2
     length = mix_input.shape[0]
     mrows = length // TP
+    more = mrows // 16
+    groups = mrows // 8 - more
     vmem = pl.BlockSpec(memory_space=pltpu.VMEM)
     hbm = pl.BlockSpec(memory_space=pltpu.HBM)
     V = pltpu.VMEM
@@ -404,10 +478,15 @@
             V((NZ, S, 8, ML), BF),
             V((NZ, S, 8, ML), BF),
             V((2, 8, CH), BF),
-            V((TP, mrows, D), BF),
-            V((2, mrows // 2, D), BF),
-            V((2, mrows, D), BF),
-            V((2, mrows // 2, D), BF),
+            V((TP, groups, 8, D), BF),
+            V((2, groups // 2, 8, D), BF),
+            V((2, groups, 8, D), BF),
+            V((2, groups // 2, 8, D), BF),
+            V((TP, 2 * more, 8, D), BF),
+            V((2, more, 8, D), BF),
+            V((2, 2 * more, 8, D), BF),
+            V((2, more, 8, D), BF),
+            V((2, more, 8, D), BF),
             V((2, ntok, n_ep * 8), BF), V((2, ntok, n_ep * 4), BF),
             dma((12,)), dma((2,)), dma((2,)),
             dma, dma((NZ,)),
@@ -415,6 +494,8 @@
             dma((2,)), dma((2, NZ)), dma((2,)), dma((2, NZ)), dma((2,)), dma((2, NZ)),
             dma, dma((NZ,)),
             dma((2,)), dma((2,)), dma((2,)), dma((2,)), dma((2,)), dma((2,)),
+            dma((2,)), dma((2,)), dma((2,)), dma((2,)), dma((2,)), dma((2,)),
+            dma((TP,)), dma((TP,)), dma, dma,
         ],
         compiler_params=pltpu.CompilerParams(
             collective_id=0, has_side_effects=True, vmem_limit_bytes=67043328 - 2 * 2 * mrows * D - 16384
@@ -428,13 +509,25 @@
 def solution(mesh):
     n_ep = mesh.shape["ep"]
     NZ, NX = (8, n_ep // 16) if n_ep >= 32 else (2, n_ep // 4)
-    order = (0, 1, 6, 3, 5, 4, 2, 7) if NZ == 8 else tuple(range(NZ))
+    if NZ == 8:
+        orders = (
+            (0, 6, 1, 2, 4, 5, 3, 7),
+            (1, 0, 2, 7, 5, 4, 6, 3),
+            (2, 3, 0, 4, 1, 6, 5, 7),
+            (3, 2, 1, 6, 4, 7, 0, 5),
+            (4, 3, 6, 2, 1, 0, 7, 5),
+            (5, 4, 3, 2, 7, 0, 1, 6),
+            (6, 4, 0, 3, 2, 1, 5, 7),
+            (7, 1, 6, 0, 3, 4, 2, 5),
+        )
+    else:
+        orders = tuple(tuple((n + c) % NZ for c in range(NZ)) for n in range(NZ))
     in_specs = (
         P("ep", "tp"), P("ep", "tp"), P("ep", "tp"), P(None, "tp"), P("tp", None), P("ep", "tp"), P(),
         P("ep", None), P("ep", None), P("ep", None, "tp"), P("ep", None, "tp"), P("ep", "tp", None),
     )
     out_specs = (P(("ep", "tp"), None), P("ep", "tp"))
     return jax.shard_map(
-        functools.partial(body, dims=(NZ, NX, order)),
+        functools.partial(body, dims=(NZ, NX, orders)),
         mesh=mesh, in_specs=in_specs, out_specs=out_specs, check_vma=False,
     )

time: 89.4 us -> 86.5 us (0.968)
  Pallas kernels: 87.3 us -> 84.4 us
    pallas_call x1, Pallas kernels: 87.3 us -> 84.4 us  [body(): pl.pallas_call(functools.partial(kernel, dims), name='step', out_shape=(V...]
where the time goes in v3:
time: 86.5 us; the launch traced here: 86.4 us
  Pallas kernels  84.4 us (98%)
  local copies, waits for them, and re-layouts  1.41 us (2%)
    pallas_call x1, Pallas kernels, body(): pl.pallas_call(functools.partial(kernel, dims), name='step', out_shape=(V...  84.4 us

profile of v3, /device:TPU:1, one launch (start us, length us, event | category | flops | bytes accessed | tf_op | source)
XLA Modules:
  0.0 86.4 jit_solution(10265020099941530568)
XLA Ops:
  0.6 84.4 %step.1 = (bf16[64,2048]{1,0:T(8,128)(2,1)S(1)}, bf16[256,512]{1,0:T(8,128)(2,1)S(1)}) custom-call(bf16[256,256]{1,0:T(8,128)(2,1)} %bg_h.1, bf16[256,256]{1,0:T(8,128)(2,1)} %cg_h.1, bf16[256,256]{1,0:T(8,128)(2,1)} %ci_h.1, f32[3,256]{1,0:T(4,128)} %taps_h.1, bf16[256,2048]{1,0:T(8,128)(2,1)} %mixw.1, bf16[256,512]{1,0:T(8,128)(2,1)} %x_h.1, ...), custom_call_target="tpu_custom_call" | custom-call | tf_op jit(solution)/shard_map/step/pallas_call | solution.py:458
  85.0 0.7 copy.16
  85.7 0.7 copy.17

commit v4 on v3

--- a/solution.py
+++ b/solution.py
@@ -189,25 +189,29 @@
     x_sems = (x1_s, x1_r, xi_s, xi_r, xa_s, xa_r)
     for tail in tails:
         tail.start()
-    begin(MS, MR1, MF, groups, m_sems, lambda q: q > 0)
-
-    handed = [
-        remote(XS.at[q, pl.ds(0, more)], XS.at[q, pl.ds(more, more)], xin_s.at[q], xin_r.at[q], ep=buddy)
-        for q in range(TP)
-    ]
-
-    @pl.when(ic == 0)
-    def _():
-        for hand in handed:
-            hand.start()
-
-    for dz in sorted(range(NZ), key=lambda n: min(n, NZ - n)):
+    def dispatch(dz):
         c = (place >> (((iz + dz) & (NZ - 1)) * 4)) & 15 if dz else 0
         for r in range(S):
             if dz + r:
                 remote(
                     out.at[dz * S + r], G.at[0, c, r], disp_s, disp_r.at[c], ep=device(dz, r // 2, r % 2)
                 ).start()
+
+    dispatch(0)
+    begin(MS, MR1, MF, groups, m_sems, lambda q: q > 0)
+
+    handed = [
+        remote(XS.at[q, pl.ds(0, more)], XS.at[q, pl.ds(more, more)], xin_s.at[q], xin_r.at[q], ep=buddy)
+        for q in range(TP)
+    ]
+
+    @pl.when(ic == 0)
+    def _():
+        for hand in handed:
+            hand.start()
+
+    for dz in sorted(range(1, NZ), key=lambda n: min(n, NZ - n)):
+        dispatch(dz)
 
     for tail in tails:
         tail.wait_recv()
@@ -367,17 +371,17 @@
         def _():
             stage_add(u - 1)
 
-        @pl.when(u >= 2)
-        def _():
-            stage_back(u - 2)
-
-        @pl.when(u == NZ - 2)
+        @pl.when(u == NZ)
         def _():
             pass_on(MS, MR1, MF, MACC, groups, m_sems)
 
             @pl.when(ic == 1)
             def _():
                 pass_on(XS, XR1, XF, XACC, 2 * more, x_sems)
+
+        @pl.when(u >= 2)
+        def _():
+            stage_back(u - 2)
 
     kept = groups * 8
     mixed[pl.ds(0, kept), :] = summed(MS, MF, groups, m_sems).reshape(kept, -1)
@@ -435,6 +439,17 @@
     def _():
         for hand in handed:
             hand.wait_send()
+
+
+def write_out(mixed, routed, mixed_out, routed_out, sems):
+    copies = [
+        pltpu.make_async_copy(mixed, mixed_out, sems.at[0]),
+        pltpu.make_async_copy(routed, routed_out, sems.at[1]),
+    ]
+    for copy in copies:
+        copy.start()
+    for copy in copies:
+        copy.wait()
 
 
 def body(mix_bgate, mix_cgate, mix_input, conv_taps, mix_out_w, moe_x, moe_gain, routes, route_w, w_gate, w_up, w_down, *, dims):
@@ -455,7 +470,7 @@
     hbm = pl.BlockSpec(memory_space=pltpu.HBM)
     V = pltpu.VMEM
     dma = pltpu.SemaphoreType.DMA
-    return pl.pallas_call(
+    results = pl.pallas_call(
         functools.partial(kernel, dims),
         name="step",
         out_shape=(
@@ -504,6 +519,15 @@
         mix_bgate, mix_cgate, mix_input, conv_taps, mix_out_w, moe_x,
         moe_gain.reshape(TP, 1, DS), routes.T, route_w.T, w_gate, w_up, w_down,
     )
+    return pl.pallas_call(
+        write_out,
+        name="write_out",
+        out_shape=tuple(jax.ShapeDtypeStruct(r.shape, BF) for r in results),
+        in_specs=[vmem, vmem],
+        out_specs=(hbm, hbm),
+        scratch_shapes=[dma((2,))],
+        compiler_params=pltpu.CompilerParams(vmem_limit_bytes=1024 * 1024),
+    )(*results)
 
 
 def solution(mesh):
@@ -511,14 +535,14 @@
     NZ, NX = (8, n_ep // 16) if n_ep >= 32 else (2, n_ep // 4)
     if NZ == 8:
         orders = (
-            (0, 6, 1, 2, 4, 5, 3, 7),
-            (1, 0, 2, 7, 5, 4, 6, 3),
-            (2, 3, 0, 4, 1, 6, 5, 7),
-            (3, 2, 1, 6, 4, 7, 0, 5),
-            (4, 3, 6, 2, 1, 0, 7, 5),
-            (5, 4, 3, 2, 7, 0, 1, 6),
-            (6, 4, 0, 3, 2, 1, 5, 7),
-            (7, 1, 6, 0, 3, 4, 2, 5),
+            (0, 1, 2, 3, 4, 5, 6, 7),
+            (1, 0, 2, 3, 5, 6, 4, 7),
+            (2, 1, 3, 0, 6, 7, 5, 4),
+            (3, 2, 1, 0, 7, 6, 5, 4),
+            (4, 3, 2, 1, 0, 7, 6, 5),
+            (5, 4, 3, 0, 1, 2, 7, 6),
+            (6, 7, 0, 1, 2, 3, 4, 5),
+            (7, 0, 1, 2, 3, 4, 5, 6),
         )
     else:
         orders = tuple(tuple((n + c) % NZ for c in range(NZ)) for n in range(NZ))

time: 86.5 us -> 85.5 us (0.988)
  local copies, waits for them, and re-layouts: 1.41 us -> 0 us
    unnamed x2 -> x0, local copies, waits for them, and re-layouts: 1.41 us -> none
    pallas_call x1, Pallas kernels: 84.4 us -> 83.1 us  [body(): pl.pallas_call(functools.partial(kernel, dims), name='step', out_shape=(V...]
where the time goes in v4:
time: 85.5 us; the launch traced here: 84.6 us
  Pallas kernels  83.9 us (98%)
    pallas_call x1, Pallas kernels, body(): pl.pallas_call(functools.partial(kernel, dims), name='step', out_shape=(V...  83.1 us

profile of v4, /device:TPU:1, one launch (start us, length us, event | category | flops | bytes accessed | tf_op | source)
XLA Modules:
  0.0 84.6 jit_solution(13188640830093337710)
XLA Ops:
  0.6 83.1 %step.1 = (bf16[64,2048]{1,0:T(8,128)(2,1)S(1)}, bf16[256,512]{1,0:T(8,128)(2,1)S(1)}) custom-call(bf16[256,256]{1,0:T(8,128)(2,1)} %bg_h.1, bf16[256,256]{1,0:T(8,128)(2,1)} %cg_h.1, bf16[256,256]{1,0:T(8,128)(2,1)} %ci_h.1, f32[3,256]{1,0:T(4,128)} %taps_h.1, bf16[256,2048]{1,0:T(8,128)(2,1)} %mixw.1, bf16[256,512]{1,0:T(8,128)(2,1)} %x_h.1, ...), custom_call_target="tpu_custom_call" | custom-call | tf_op jit(solution)/shard_map/step/pallas_call | solution.py:473
  83.8 0.8 write_out.1

commit v5 on v4

--- a/solution.py
+++ b/solution.py
@@ -46,7 +46,7 @@
     halo, MS, MR1, MF, MACC, XS, XR1, XF, XACC, XO, pick_a, pick_b,
     wsem, halo_s, halo_r, disp_s, disp_r, gd_s, gd_r, gr_s, gr_r,
     r1_s, r1_r, fi_s, fi_r, fa_s, fa_r, back_s, back_r,
-    m1_s, m1_r, mi_s, mi_r, ma_s, ma_r, x1_s, x1_r, xi_s, xi_r, xa_s, xa_r, xin_s, xin_r, xo_s, xo_r,
+    m1_s, m1_r, mi_s, mi_r, ma_s, ma_r, x1_s, x1_r, xi_s, xi_r, xa_s, xa_r, xin_s, xin_r, xo_s, xo_r, news,
 ):
     NZ, NX, orders = dims
     S = NX * 2
@@ -92,12 +92,28 @@
     def greet(ep, tp):
         pl.semaphore_signal(barrier, inc=1, device_id=(ep, tp), device_id_type=pl.DeviceIdType.MESH)
 
-    for dz in sorted(range(NZ), key=lambda n: -min(n, NZ - n)):
-        for r in range(S):
-            if dz + r:
-                greet(device(dz, r // 2, r % 2), y)
+    greet((i + n_ep - 1) & (n_ep - 1), y)
+    beside = (device(1, 0, 0), device(NZ - 1, 0, 0))
+    for other in beside:
+        greet(other, y)
+    for r in range(1, S):
+        greet(device(0, r // 2, r % 2), y)
     for _, other in sides:
         greet(i, other)
+
+    def tell(n):
+        for d, other in enumerate(beside):
+            pl.semaphore_signal(
+                news.at[n, d], inc=1, device_id=(other, y), device_id_type=pl.DeviceIdType.MESH
+            )
+
+    def reach(n):
+        for d in range(2):
+            pl.semaphore_wait(news.at[n, d], 1)
+        if n + 1 < NZ // 2:
+            tell(n + 1)
+        for dz in sorted({n + 1, NZ - n - 1}):
+            dispatch(dz)
 
     loads = [
         pltpu.make_async_copy(src, dst, wsem.at[n])
@@ -160,7 +176,8 @@
             MS[q] = product[:groups]
         XS[q, pl.ds(0, more)] = product[groups:]
 
-    pl.semaphore_wait(barrier, n_ep - 1 + 2)
+    pl.semaphore_wait(barrier, S - 1 + 5)
+    tell(0)
 
     ntail = cg.shape[0] - 8
     tails = [
@@ -210,9 +227,7 @@
         for hand in handed:
             hand.start()
 
-    for dz in sorted(range(1, NZ), key=lambda n: min(n, NZ - n)):
-        dispatch(dz)
-
+    reach(0)
     for tail in tails:
         tail.wait_recv()
     prev = halo[0].astype(F32) * halo[1].astype(F32)
@@ -241,12 +256,17 @@
         return (own[y].astype(F32) + last[0].astype(F32) + last[1].astype(F32)).astype(BF)
 
     begin(MS, MR1, MF, groups, m_sems, lambda q: q == 0)
+    if NZ > 2:
+        reach(1)
 
     @pl.when(ic == 1)
     def _():
         for hand in handed:
             hand.wait_recv()
         begin(XS, XR1, XF, 2 * more, x_sems, lambda q: q >= 0)
+
+    if NZ > 4:
+        reach(2)
 
     loads[7].wait()
     loads[8].wait()
@@ -262,6 +282,9 @@
         pick_a[q] = jnp.where(ga == cols[:, q : q + 1].astype(jnp.int32), 1.0, 0.0).astype(BF)
         pick_b[q] = jnp.where(gb == cols[:, 2 + q : 3 + q].astype(jnp.int32), 1.0, 0.0).astype(BF)
     share = [cols[:, 4 + q : 5 + q] for q in range(2)]
+
+    if NZ > 6:
+        reach(3)
 
     def stage_direct(c):
         @pl.when(c == 0)
@@ -510,7 +533,7 @@
             dma, dma((NZ,)),
             dma((2,)), dma((2,)), dma((2,)), dma((2,)), dma((2,)), dma((2,)),
             dma((2,)), dma((2,)), dma((2,)), dma((2,)), dma((2,)), dma((2,)),
-            dma((TP,)), dma((TP,)), dma, dma,
+            dma((TP,)), dma((TP,)), dma, dma, pltpu.SemaphoreType.REGULAR((NZ // 2, 2)),
         ],
         compiler_params=pltpu.CompilerParams(
             collective_id=0, has_side_effects=True, vmem_limit_bytes=67043328 - 2 * 2 * mrows * D - 16384

time: 85.5 us -> 84 us (0.982); the launches traced: 84.6 us -> 83.9 us
  no operation moved by 1% of the time
where the time goes in v5:
time: 84 us; the launch traced here: 83.9 us
  Pallas kernels  83.3 us (99%)
    pallas_call x1, Pallas kernels, body(): pl.pallas_call(functools.partial(kernel, dims), name='step', out_shape=(V...  82.5 us

profile of v5, /device:TPU:1, one launch (start us, length us, event | category | flops | bytes accessed | tf_op | source)
XLA Modules:
  0.0 83.9 jit_solution(17337279559073128944)
XLA Ops:
  0.6 82.5 %step.1 = (bf16[64,2048]{1,0:T(8,128)(2,1)S(1)}, bf16[256,512]{1,0:T(8,128)(2,1)S(1)}) custom-call(bf16[256,256]{1,0:T(8,128)(2,1)} %bg_h.1, bf16[256,256]{1,0:T(8,128)(2,1)} %cg_h.1, bf16[256,256]{1,0:T(8,128)(2,1)} %ci_h.1, f32[3,256]{1,0:T(4,128)} %taps_h.1, bf16[256,2048]{1,0:T(8,128)(2,1)} %mixw.1, bf16[256,512]{1,0:T(8,128)(2,1)} %x_h.1, ...), custom_call_target="tpu_custom_call" | custom-call | tf_op jit(solution)/shard_map/step/pallas_call | solution.py:496
  83.1 0.8 write_out.1

commit v6 on v5

--- a/solution.py
+++ b/solution.py
@@ -282,9 +282,6 @@
         pick_a[q] = jnp.where(ga == cols[:, q : q + 1].astype(jnp.int32), 1.0, 0.0).astype(BF)
         pick_b[q] = jnp.where(gb == cols[:, 2 + q : 3 + q].astype(jnp.int32), 1.0, 0.0).astype(BF)
     share = [cols[:, 4 + q : 5 + q] for q in range(2)]
-
-    if NZ > 6:
-        reach(3)
 
     def stage_direct(c):
         @pl.when(c == 0)
@@ -385,6 +382,9 @@
         @pl.when(u < NZ - 3)
         def _():
             stage_direct(u + 3)
+
+        if NZ > 6:
+            pl.when(u == -3)(lambda: reach(3))
 
         @pl.when((u >= 0) & (u < NZ))
         def _():

time: 84 us -> 84 us (level)
  no operation moved by 1% of the time
where the time goes in v6:
time: 84 us; the launch traced here: 83.9 us
  Pallas kernels  83.3 us (99%)
    pallas_call x1, Pallas kernels, body(): pl.pallas_call(functools.partial(kernel, dims), name='step', out_shape=(V...  82.5 us

profile of v6, /device:TPU:1, one launch (start us, length us, event | category | flops | bytes accessed | tf_op | source)
XLA Modules:
  0.0 83.9 jit_solution(6067495330832563148)
XLA Ops:
  0.6 82.5 %step.1 = (bf16[64,2048]{1,0:T(8,128)(2,1)S(1)}, bf16[256,512]{1,0:T(8,128)(2,1)S(1)}) custom-call(bf16[256,256]{1,0:T(8,128)(2,1)} %bg_h.1, bf16[256,256]{1,0:T(8,128)(2,1)} %cg_h.1, bf16[256,256]{1,0:T(8,128)(2,1)} %ci_h.1, f32[3,256]{1,0:T(4,128)} %taps_h.1, bf16[256,2048]{1,0:T(8,128)(2,1)} %mixw.1, bf16[256,512]{1,0:T(8,128)(2,1)} %x_h.1, ...), custom_call_target="tpu_custom_call" | custom-call | tf_op jit(solution)/shard_map/step/pallas_call | solution.py:496
  83.1 0.8 write_out.1
